TPU v7x, 32 devices: a whole 2x2x4 slice. The times are simulated.
32 devices in a mesh: sp: 16 (over z, x, core), tp: 2 (over y).
Axes of the slice: x: 2, y: 2, z: 4, core: 2. Of those that a mesh axis runs over, the one named last changes fastest.
Arguments:
- stream: bfloat16 [6144, 2048], P(('sp', 'tp')), may hold values from -6 to 6
- query_narrow: bfloat16 [6144, 512], P('sp', 'tp'), may hold values from -6 to 6
- key_narrow: bfloat16 [6144, 512], P('sp', 'tp'), may hold values from -6.5 to 6.5
- query_wide: bfloat16 [6144, 1024], P('sp', 'tp'), may hold values from -6 to 6
- key_wide: bfloat16 [6144, 1024], P('sp', 'tp'), may hold values from -6.5 to 6.5
- values: bfloat16 [6144, 2, 1024], P('sp', None, 'tp'), may hold values from -6 to 6
- out_gate: bfloat16 [6144, 2, 1024], P('sp', None, 'tp'), may hold values from -6 to 6
- out_weight: bfloat16 [2, 1024, 2048], P(None, 'tp'), may hold values from -0.125 to 0.125
- norm_gain: float32 [2048], replicated, may hold values from 0.1 to 1.9
- mlp_gate: bfloat16 [2048, 5632], P('sp', 'tp'), may hold values from -0.125 to 0.125
- mlp_up: bfloat16 [2048, 5632], P('sp', 'tp'), may hold values from -0.125 to 0.125
- mlp_down: bfloat16 [5632, 2048], P('tp', 'sp'), may hold values from -0.15625 to 0.15625
- log_decay: float32 [2, 2, 8], P(None, None, 'tp'), as said below
Outputs:
- layer_out: bfloat16 [6144, 2048], P(('sp', 'tp'))
Inputs may be any that keep to these rules, and one draw needn't show every extreme that they name: `log_decay`: every entry is negative, with magnitude at least 0.5 / 6144.
All inputs are finite; a program needn't handle non-finite values.
Results may differ from a plain program's by a relative error of at most 0.013.
Values may be sent and summed in bfloat16 or wider, within the bound.
A program may use at most 128 MiB of HBM per device.

v0:
```python
import jax
import jax.numpy as jnp
from jax import lax
from jax.sharding import PartitionSpec as P

BLOCK = 128


NORM_EPSILON = 1e-06
ROPE_BASE = 10000.0


def prefix(value, axis, join, neutral, backward):
    count, mine = (lax.axis_size(axis), lax.axis_index(axis))
    pieces = jax.tree.map(lambda part: lax.all_gather(part, axis), value)
    if backward:
        pieces = jax.tree.map(lambda part: part[::-1], pieces)
        mine = count - 1 - mine
    subtotal = jax.tree.map(
        lambda part, zero: jnp.full_like(part, 0) + jnp.asarray(zero, part.dtype), value, neutral
    )

    def hop(position, subtotal):
        longer = join(subtotal, jax.tree.map(lambda part: part[position], pieces))
        return jax.tree.map(lambda new, old: jnp.where(position < mine, new, old), longer, subtotal)

    return lax.fori_loop(0, count - 1, hop, subtotal)


def rotate(block_in, positions):
    half_size = block_in.shape[-1] // 2
    frequencies = jnp.power(ROPE_BASE, -(jnp.arange(half_size, dtype=jnp.float32) / half_size))
    angles = positions[:, None] * frequencies[None, :]
    cosine = jnp.cos(angles)[:, None, :]
    sine_table = jnp.sin(angles)[:, None, :]
    first_half = block_in[..., :half_size]
    second_half = block_in[..., half_size:]
    return jnp.concatenate(
        [
            first_half * cosine - second_half * sine_table,
            first_half * sine_table + second_half * cosine,
        ],
        -1,
    )


def decay_tables(rate_fwd, rate_bwd, block_len):
    position = jnp.arange(block_len, dtype=jnp.float32)
    offset = position[:, None] - position[None, :]
    forward_part = jnp.exp(rate_fwd[:, None, None] * jnp.maximum(offset, 0.0)[None])
    backward_part = jnp.exp(rate_bwd[:, None, None] * jnp.maximum(-offset, 0.0)[None])
    inner = jnp.where(
        offset[None] > 0, forward_part, jnp.where(offset[None] < 0, backward_part, 2.0)
    )
    keep_fwd = jnp.exp(rate_fwd[:, None] * (block_len - 1.0 - position)[None, :])
    keep_bwd = jnp.exp(rate_bwd[:, None] * position[None, :])
    reach_fwd = jnp.exp(rate_fwd[:, None] * (position + 1.0)[None, :])
    reach_bwd = jnp.exp(rate_bwd[:, None] * (block_len - position)[None, :])
    return (inner, keep_fwd, keep_bwd, reach_fwd, reach_bwd)


def local_part(query_rows, key_rows, value_rows, rate_fwd, rate_bwd, positions):
    length = query_rows.shape[0]
    head_count = rate_fwd.shape[0]
    key_size = query_rows.shape[1] // head_count
    value_size = value_rows.shape[1] // head_count
    block_count = length // BLOCK
    highest_precision = lax.Precision.HIGHEST
    query_rot = rotate(
        query_rows.astype(jnp.float32).reshape(length, head_count, key_size), positions
    ).astype(jnp.bfloat16)
    key_rot = (
        rotate(key_rows.astype(jnp.float32).reshape(length, head_count, key_size), positions)
        * key_size ** (-0.5)
    ).astype(jnp.bfloat16)
    query_blk = query_rot.reshape(block_count, BLOCK, head_count, key_size)
    key_blk = key_rot.reshape(block_count, BLOCK, head_count, key_size)
    value_blk = value_rows.reshape(block_count, BLOCK, head_count, value_size)
    inner, keep_fwd, keep_bwd, reach_fwd, reach_bwd = decay_tables(rate_fwd, rate_bwd, BLOCK)
    scores = jnp.einsum("cthk,cshk->chts", query_blk, key_blk, preferred_element_type=jnp.float32)
    weights = (scores * inner[None]).astype(jnp.bfloat16)
    inside = jnp.einsum("chts,cshv->cthv", weights, value_blk, preferred_element_type=jnp.float32)
    key_wide32 = key_blk.astype(jnp.float32)
    value_wide32 = value_blk.astype(jnp.float32)
    update_fwd = jnp.einsum(
        "cshk,cshv->chkv",
        key_wide32 * keep_fwd.T[None, :, :, None],
        value_wide32,
        precision=highest_precision,
    )
    update_bwd = jnp.einsum(
        "cshk,cshv->chkv",
        key_wide32 * keep_bwd.T[None, :, :, None],
        value_wide32,
        precision=highest_precision,
    )
    block_index = jnp.arange(block_count, dtype=jnp.float32)
    device_fwd = jnp.einsum(
        "qp,pqjl->qjl",
        jnp.exp(rate_fwd[:, None] * (BLOCK * (block_count - 1.0 - block_index))[None, :]),
        update_fwd,
        precision=highest_precision,
    )
    device_bwd = jnp.einsum(
        "qp,pqjl->qjl",
        jnp.exp(rate_bwd[:, None] * (BLOCK * block_index)[None, :]),
        update_bwd,
        precision=highest_precision,
    )
    span_fwd = jnp.exp(rate_fwd * length)
    span_bwd = jnp.exp(rate_bwd * length)
    pieces = (query_blk, inside, update_fwd, update_bwd, reach_fwd, reach_bwd)
    return (pieces, device_fwd, device_bwd, span_fwd, span_bwd)


def finish(pieces, enter_fwd, enter_bwd, rate_fwd, rate_bwd, gate_rows):
    query_blk, inside, update_fwd, update_bwd, reach_fwd, reach_bwd = pieces
    block_count = inside.shape[0]
    highest_precision = lax.Precision.HIGHEST
    block_index = jnp.arange(block_count, dtype=jnp.float32)
    block_lag = block_index[:, None] - block_index[None, :] - 1.0
    earlier_weights = jnp.where(
        block_lag[None] >= 0,
        jnp.exp(rate_fwd[:, None, None] * BLOCK * jnp.maximum(block_lag, 0.0)[None]),
        0.0,
    )
    later_weights = jnp.where(
        block_lag.T[None] >= 0,
        jnp.exp(rate_bwd[:, None, None] * BLOCK * jnp.maximum(block_lag.T, 0.0)[None]),
        0.0,
    )
    start_fwd = (
        jnp.einsum("hcd,dhkv->chkv", earlier_weights, update_fwd, precision=highest_precision)
        + jnp.exp(rate_fwd[None, :] * BLOCK * block_index[:, None])[:, :, None, None]
        * enter_fwd[None]
    )
    start_bwd = (
        jnp.einsum("hcd,dhkv->chkv", later_weights, update_bwd, precision=highest_precision)
        + jnp.exp(rate_bwd[None, :] * BLOCK * (block_count - 1.0 - block_index)[:, None])[
            :, :, None, None
        ]
        * enter_bwd[None]
    )
    query_wide32 = query_blk.astype(jnp.float32)
    carried_state = jnp.einsum(
        "cthk,chkv->cthv",
        query_wide32 * reach_fwd.T[None, :, :, None],
        start_fwd,
        precision=highest_precision,
    ) + jnp.einsum(
        "cthk,chkv->cthv",
        query_wide32 * reach_bwd.T[None, :, :, None],
        start_bwd,
        precision=highest_precision,
    )
    combined = inside + carried_state
    length = block_count * BLOCK
    combined = combined.reshape(length, combined.shape[2], combined.shape[3])
    mean_value = jnp.mean(combined, -1, keepdims=True)
    centred = combined - mean_value
    variance = jnp.mean(centred * centred, -1, keepdims=True)
    scaled = centred * lax.rsqrt(variance + NORM_EPSILON)
    gated = jax.nn.silu(gate_rows.astype(jnp.float32)).reshape(combined.shape) * scaled
    return gated.reshape(length, -1).astype(jnp.bfloat16)


def rms_scale(rows_in, gain):
    widened = rows_in.astype(jnp.float32)
    return (
        widened * lax.rsqrt(jnp.mean(widened * widened, -1, keepdims=True) + NORM_EPSILON) * gain
    ).astype(jnp.bfloat16)


def chain_step(earlier, later_part):
    return (
        earlier[0] * later_part[2][:, None, None] + later_part[0],
        earlier[1] * later_part[3][:, None, None] + later_part[1],
        earlier[2] * later_part[2],
        earlier[3] * later_part[3],
    )


def body(
    stream,
    query_narrow,
    key_narrow,
    query_wide,
    key_wide,
    values,
    out_gate,
    out_weight,
    norm_gain,
    mlp_gate,
    mlp_up,
    mlp_down,
    log_decay,
):
    full_gate, full_up, full_down = (
        lax.all_gather(mlp_gate, "sp", axis=0, tiled=True),
        lax.all_gather(mlp_up, "sp", axis=0, tiled=True),
        lax.all_gather(mlp_down, "sp", axis=1, tiled=True),
    )
    length = query_narrow.shape[0]
    positions = (lax.axis_index("sp") * length + jnp.arange(length, dtype=jnp.int32)).astype(
        jnp.float32
    )
    narrow_pieces, narrow_fwd, narrow_bwd, narrow_span_fwd, narrow_span_bwd = local_part(
        query_narrow, key_narrow, values[:, 0], log_decay[0, 0], log_decay[1, 0], positions
    )
    wide_pieces, wide_fwd, wide_bwd, wide_span_fwd, wide_span_bwd = local_part(
        query_wide, key_wide, values[:, 1], log_decay[0, 1], log_decay[1, 1], positions
    )
    identity = (
        jnp.zeros_like(narrow_fwd),
        jnp.zeros_like(wide_fwd),
        jnp.ones_like(narrow_span_fwd),
        jnp.ones_like(wide_span_fwd),
    )
    enter_fwd = prefix(
        (narrow_fwd, wide_fwd, narrow_span_fwd, wide_span_fwd), "sp", chain_step, identity, False
    )
    enter_bwd = prefix(
        (narrow_bwd, wide_bwd, narrow_span_bwd, wide_span_bwd), "sp", chain_step, identity, True
    )
    narrow_out = finish(
        narrow_pieces, enter_fwd[0], enter_bwd[0], log_decay[0, 0], log_decay[1, 0], out_gate[:, 0]
    )
    wide_out = finish(
        wide_pieces, enter_fwd[1], enter_bwd[1], log_decay[0, 1], log_decay[1, 1], out_gate[:, 1]
    )
    proj_rows = lax.psum_scatter(
        jnp.dot(narrow_out, out_weight[0], preferred_element_type=jnp.float32)
        + jnp.dot(wide_out, out_weight[1], preferred_element_type=jnp.float32),
        "tp",
        scatter_dimension=0,
        tiled=True,
    )
    middle = (stream.astype(jnp.float32) + proj_rows).astype(jnp.bfloat16)
    normed = lax.all_gather(rms_scale(middle, norm_gain), "tp", axis=0, tiled=True)
    gate_act = jnp.dot(normed, full_gate, preferred_element_type=jnp.float32)
    up_act = jnp.dot(normed, full_up, preferred_element_type=jnp.float32)
    hidden = (jax.nn.silu(gate_act) * up_act).astype(jnp.bfloat16)
    down_rows = lax.psum_scatter(
        jnp.dot(hidden, full_down, preferred_element_type=jnp.float32).astype(jnp.bfloat16),
        "tp",
        scatter_dimension=0,
        tiled=True,
    ).astype(jnp.float32)
    return (middle.astype(jnp.float32) + 0.5 * down_rows).astype(jnp.bfloat16)


def solution(mesh):
    return jax.shard_map(
        body,
        mesh=mesh,
        in_specs=(
            P(("sp", "tp"), None),
            P("sp", "tp"),
            P("sp", "tp"),
            P("sp", "tp"),
            P("sp", "tp"),
            P("sp", None, "tp"),
            P("sp", None, "tp"),
            P(None, "tp", None),
            P(),
            P("sp", "tp"),
            P("sp", "tp"),
            P("tp", "sp"),
            P(None, None, "tp"),
        ),
        out_specs=P(("sp", "tp"), None),
        check_vma=False,
    )
```

profile of v0, /device:TPU:0, one launch (start us, length us, event | category | flops | bytes accessed | tf_op | source)
XLA Modules:
  0.0 703.9 jit_solution(9049273779724230727)
XLA Ops:
  10.3 4.8 slice_reduce_fusion
  25.2 3.5 fusion.28
  32.0 2.9 fusion.31
  39.8 24.3 %all-gather.4 = f32[16,1,4]{2,1,0:T(1,128)} all-gather(f32[1,1,4]{2,1,0:T(1,128)} %get-tuple-element.461), channel_id=6, replica_groups=mesh['sp'=16,'tp'=2] {'sp'}, dimensions={0}, use_global_device_ids=true | all-gather | bytes 272 | tf_op jit(solution)/shard_map/all_gather | solution.py:15
  68.2 18.2 %all-gather.6 = f32[16,1,4]{2,1,0:T(1,128)} all-gather(f32[1,1,4]{2,1,0:T(1,128)} %get-tuple-element.465), channel_id=8, replica_groups=mesh['sp'=16,'tp'=2] {'sp'}, dimensions={0}, use_global_device_ids=true | all-gather | bytes 272 | tf_op jit(solution)/shard_map/all_gather | solution.py:15
  90.4 20.3 %all-gather = f32[16,1,4]{2,1,0:T(1,128)} all-gather(f32[1,1,4]{2,1,0:T(1,128)} %get-tuple-element.460), channel_id=2, replica_groups=mesh['sp'=16,'tp'=2] {'sp'}, dimensions={0}, use_global_device_ids=true | all-gather | bytes 272 | tf_op jit(solution)/shard_map/all_gather | solution.py:15
  110.7 18.4 %all-gather.2 = f32[16,1,4]{2,1,0:T(1,128)} all-gather(f32[1,1,4]{2,1,0:T(1,128)} %get-tuple-element.466), channel_id=4, replica_groups=mesh['sp'=16,'tp'=2] {'sp'}, dimensions={0}, use_global_device_ids=true | all-gather | bytes 272 | tf_op jit(solution)/shard_map/all_gather | solution.py:15
  130.8 1.9 copy.101
  134.4 1.9 copy.102
  139.4 3.9 fusion.133
  145.7 3.2 rev.13
  148.9 4.8 rev.15
  153.7 41.5 %while.33 = (s32[]{:T(128)}, f32[4,64,128]{2,1,0:T(8,128)S(1)}, f32[4,128,128]{2,1,0:T(8,128)S(1)}, s32[]{:T(128)}, f32[16,4]{1,0:T(8,128)}, /*index=5*/f32[16,4...) while((s32[]{:T(128)}, f32[4,64,128]{2,1,0:T(8,128)S(1)}, ...), condition=%wide.region_3.4_spmd.clone, body=%wide.region_2.3_spmd.clone.sunk | while | flops 393220 | bytes 1179879 | solution.py:27
  195.2 14.8 %all-gather.27.cloned.1.call-done = f32[64,128,128]{2,1,0:T(8,128)} async-done(((f32[4,128,128]{2,1,0:T(8,128)}), f32[64,128,128]{2,1,0:T(8,128)}) %all-gather.27.cloned.1.call-update) | async-done | bytes 4194320 | tf_op jit(solution)/shard_map/all_gather | solution.py:15
  210.1 41.8 %while.32 = (s32[]{:T(128)}, f32[4,64,128]{2,1,0:T(8,128)S(1)}, f32[4,128,128]{2,1,0:T(8,128)S(1)}, s32[]{:T(128)}, f32[16,4]{1,0:T(8,128)}, /*index=5*/f32[16,4...) while((s32[]{:T(128)}, f32[4,64,128]{2,1,0:T(8,128)S(1)}, ...), condition=%wide.region_1.2_spmd.clone, body=%wide.region_0.1_spmd.clone.sunk | while | flops 393220 | bytes 1179879 | solution.py:27
  251.9 3.2 fusion.18
  255.1 3.1 fusion.19
  260.0 2.6 fusion.23
  268.3 2.4 sub.296
  274.7 2.3 fusion.58
  277.0 2.3 fusion.20
  283.7 3.0 fusion.10
  287.6 2.7 convolution_add_fusion
  290.4 41.9 %reduce-scatter.3.cloned.1.call-done = f32[192,2048]{1,0:T(8,128)} async-done(((f32[384,2048]{1,0:T(8,128)}), f32[192,2048]{1,0:T(8,128)}) %reduce-scatter.3.cloned.1.call-update) | async-done | bytes 1572880 | tf_op jit(solution)/shard_map/reduce_scatter | solution.py:231
  337.7 24.9 %all-gather.17.cloned.1.call-done = bf16[384,2048]{1,0:T(8,128)(2,1)} async-done(((bf16[192,2048]{1,0:T(8,128)(2,1)}), bf16[384,2048]{1,0:T(8,128)(2,1)}) %all-gather.17.cloned.1.call-update) | async-done | bytes 1572880 | tf_op jit(solution)/shard_map/all_gather | solution.py:239
  362.6 96.3 %all-gather.19.cloned.1.call-done = bf16[2048,2816]{1,0:T(8,128)(2,1)} async-done(((bf16[128,2816]{1,0:T(8,128)(2,1)}), bf16[2048,2816]{1,0:T(8,128)(2,1)}) %all-gather.19.cloned.1.call-update) | async-done | bytes 11534352 | tf_op jit(solution)/shard_map/all_gather | solution.py:199
  458.9 11.4 %fusion.138 = f32[384,2816]{1,0:T(8,128)} fusion(bf16[384,2048]{1,0:T(8,128)(2,1)} %all-gather.17.cloned.1.call-done, bf16[2048,2816]{1,0:T(8,128)(2,1)} %all-gather.19.cloned.1.call-done), kind=kOutput, calls=%fused_computation.238 | convolution fusion | flops 4429185024 | bytes 17432576 | tf_op jit(solution)/shard_map/dot_general | solution.py:240
  470.3 83.1 %all-gather.21.cloned.1.call-done = bf16[2048,2816]{1,0:T(8,128)(2,1)} async-done(((bf16[128,2816]{1,0:T(8,128)(2,1)}), bf16[2048,2816]{1,0:T(8,128)(2,1)}) %all-gather.21.cloned.1.call-update) | async-done | bytes 11534352 | tf_op jit(solution)/shard_map/all_gather | solution.py:200
  553.4 97.3 %all-gather.23.cloned.1.call-done = bf16[2816,2048]{1,0:T(8,128)(2,1)} async-done(((bf16[2816,128]{1,0:T(8,128)(2,1)}), bf16[2816,2048]{1,0:T(8,128)(2,1)}) %all-gather.23.cloned.1.call-update) | async-done | bytes 11534352 | tf_op jit(solution)/shard_map/all_gather | solution.py:201
  650.8 19.3 %convolution_convert_fusion = bf16[384,2048]{1,0:T(8,128)(2,1)} fusion(bf16[2816,2048]{1,0:T(8,128)(2,1)} %all-gather.23.cloned.1.call-done, bf16[384,2048]{1,0:T(8,128)(2,1)S(1)} %copy-done.53, bf16[2048,2816]{1,0:T(8,128)(2,1)} %all-gather.21.cloned.1.call-done, f32[384,2816]{1,0:T(8,128)} %fusion.138), kind=kOutput, calls=%fused_computation.19 | convolution fusion | flops 8865644544 | bytes 30539776 | tf_op jit(solution)/shard_map/dot_general | solution.py:244
  670.1 24.5 %reduce-scatter.5.cloned.1.call-done = bf16[192,2048]{1,0:T(8,128)(2,1)} async-done(((bf16[384,2048]{1,0:T(8,128)(2,1)}), bf16[192,2048]{1,0:T(8,128)(2,1)}) %reduce-scatter.5.cloned.1.call-update) | async-done | bytes 786448 | tf_op jit(solution)/shard_map/reduce_scatter | solution.py:243
  694.6 2.3 fusion.17
  (311 shorter events, 142.5 us)
Async XLA Ops:
  6.5 139.2 %all-gather.29.cloned.1.call-start = ((), (), s32[]{:S(2)}) async-start(), calls=%async_computation.10 | async-start | bytes 2228224 | tf_op jit(solution)/shard_map/all_gather | solution.py:15
  8.0 9.0 %copy-start.35 = (f32[4]{0:T(128)}, f32[4]{0:T(128)S(1)}, u32[]{:S(2)}) copy-start(f32[4]{0:T(128)S(1)} %get-tuple-element.459) | copy-start | bytes 52
  8.0 9.0 %copy-start.37 = (f32[4]{0:T(128)}, f32[4]{0:T(128)S(1)}, u32[]{:S(2)}) copy-start(f32[4]{0:T(128)S(1)} %get-tuple-element.462) | copy-start | bytes 52
  8.0 9.0 %copy-start.39 = (f32[4]{0:T(128)}, f32[4]{0:T(128)S(1)}, u32[]{:S(2)}) copy-start(f32[4]{0:T(128)S(1)} %get-tuple-element.463) | copy-start | bytes 52
  8.0 9.0 %copy-start.41 = (f32[4]{0:T(128)}, f32[4]{0:T(128)S(1)}, u32[]{:S(2)}) copy-start(f32[4]{0:T(128)S(1)} %get-tuple-element.464) | copy-start | bytes 52
  16.3 12.5 %copy-start.8 = (f32[3,128,4,32]{1,3,2,0:T(8,128)}, f32[3,128,4,32]{1,3,2,0:T(8,128)S(1)}, u32[]{:S(2)}) copy-start(f32[3,128,4,32]{1,3,2,0:T(8,128)S(1)} %get-tuple-element.485) | copy-start | bytes 589828
  16.3 12.5 %copy-start.10 = (f32[3,128,4,32]{1,3,2,0:T(8,128)}, f32[3,128,4,32]{1,3,2,0:T(8,128)S(1)}, u32[]{:S(2)}) copy-start(f32[3,128,4,32]{1,3,2,0:T(8,128)S(1)} %get-tuple-element.486) | copy-start | bytes 589828
  20.7 128.2 %all-gather.31.cloned.1.call-start = ((), (), s32[]{:S(2)}) async-start(), calls=%async_computation.11 | async-start | bytes 4456448 | tf_op jit(solution)/shard_map/all_gather | solution.py:15
  25.2 9.8 %copy-start.34 = (f32[2,2,4]{2,1,0:T(2,128)S(1)}, f32[2,2,4]{2,1,0:T(2,128)}, u32[]{:S(2)}) copy-start(f32[2,2,4]{2,1,0:T(2,128)} %param.29) | copy-start | bytes 196
  28.7 166.5 %all-gather.25.cloned.1.call-start = ((), (), s32[]{:S(2)}) async-start(), calls=%async_computation.8 | async-start | bytes 2228224 | tf_op jit(solution)/shard_map/all_gather | solution.py:15
  31.1 179.0 %all-gather.27.cloned.1.call-start = ((), (), s32[]{:S(2)}) async-start(), calls=%async_computation.9 | async-start | bytes 4456448 | tf_op jit(solution)/shard_map/all_gather | solution.py:15
  34.9 297.5 %reduce-scatter.3.cloned.1.call-start = ((), (), s32[]{:S(2)}) async-start(), calls=%async_computation.2 | async-start | bytes 4718592 | tf_op jit(solution)/shard_map/reduce_scatter | solution.py:231
  136.4 8.3 %copy-start.23 = (f32[128,128]{1,0:T(8,128)S(1)}, f32[128,128]{1,0:T(8,128)}, u32[]{:S(2)}) copy-start(f32[128,128]{1,0:T(8,128)} %get-tuple-element.494) | copy-start | bytes 196612
  136.4 8.3 %copy-start.24 = (f32[128,128]{1,0:T(8,128)S(1)}, f32[128,128]{1,0:T(8,128)}, u32[]{:S(2)}) copy-start(f32[128,128]{1,0:T(8,128)} %get-tuple-element.495) | copy-start | bytes 196612
  136.4 8.3 %copy-start.25 = (pred[128,128]{1,0:T(8,128)(4,1)S(1)}, pred[128,128]{1,0:T(8,128)(4,1)}, u32[]{:S(2)}) copy-start(pred[128,128]{1,0:T(8,128)(4,1)} %get-tuple-element.497) | copy-start | bytes 49156
  136.4 8.2 %copy-start.36 = (f32[4]{0:T(128)S(1)}, f32[4]{0:T(128)}, u32[]{:S(2)}) copy-start(f32[4]{0:T(128)} %copy-done.35) | copy-start | bytes 52
  136.4 8.2 %copy-start.38 = (f32[4]{0:T(128)S(1)}, f32[4]{0:T(128)}, u32[]{:S(2)}) copy-start(f32[4]{0:T(128)} %copy-done.37) | copy-start | bytes 52
  136.4 8.2 %copy-start.40 = (f32[4]{0:T(128)S(1)}, f32[4]{0:T(128)}, u32[]{:S(2)}) copy-start(f32[4]{0:T(128)} %copy-done.39) | copy-start | bytes 52
  136.4 8.2 %copy-start.42 = (f32[4]{0:T(128)S(1)}, f32[4]{0:T(128)}, u32[]{:S(2)}) copy-start(f32[4]{0:T(128)} %copy-done.41) | copy-start | bytes 52
  195.2 56.7 %copy-start.27 = (f32[3,3]{1,0:T(4,128)S(1)}, f32[3,3]{1,0:T(4,128)}, u32[]{:S(2)}) copy-start(f32[3,3]{1,0:T(4,128)} %fusion.116) | copy-start | bytes 112
  210.1 45.0 %copy-start.26 = (f32[3,3]{1,0:T(4,128)S(1)}, f32[3,3]{1,0:T(4,128)}, u32[]{:S(2)}) copy-start(f32[3,3]{1,0:T(4,128)} %fusion.118) | copy-start | bytes 112
  251.9 8.0 %copy-start.43 = (f32[128,4]{0,1:T(4,128)S(1)}, f32[128,4]{0,1:T(4,128)}, u32[]{:S(2)}) copy-start(f32[128,4]{0,1:T(4,128)} %get-tuple-element.467) | copy-start | bytes 6148
  267.0 7.7 %copy-start.30 = (f32[128,4]{0,1:T(4,128)S(1)}, f32[128,4]{0,1:T(4,128)}, u32[]{:S(2)}) copy-start(f32[128,4]{0,1:T(4,128)} %get-tuple-element.487) | copy-start | bytes 6148
  268.3 8.7 %copy-start.29 = (f32[128,4]{0,1:T(4,128)S(1)}, f32[128,4]{0,1:T(4,128)}, u32[]{:S(2)}) copy-start(f32[128,4]{0,1:T(4,128)} %get-tuple-element.469) | copy-start | bytes 6148
  290.4 42.0 %copy-start.19 = (bf16[192,2048]{1,0:T(8,128)(2,1)S(1)}, bf16[192,2048]{1,0:T(8,128)(2,1)}, u32[]{:S(2)}) copy-start(bf16[192,2048]{1,0:T(8,128)(2,1)} %param.17) | copy-start | bytes 2359300
  290.4 43.7 %copy-start.28 = (f32[2048]{0:T(1024)S(1)}, f32[2048]{0:T(1024)}, u32[]{:S(2)}) copy-start(f32[2048]{0:T(1024)} %param.25) | copy-start | bytes 24580
  290.4 72.2 %all-gather.17.cloned.1.call-start = ((), (), s32[]{:S(2)}) async-start(), calls=%async_computation.3 | async-start | bytes 2359296 | tf_op jit(solution)/shard_map/all_gather | solution.py:239
  335.2 123.6 %all-gather.19.cloned.1.call-start = ((), (), s32[]{:S(2)}) async-start(), calls=%async_computation.4 | async-start | bytes 12255232 | tf_op jit(solution)/shard_map/all_gather | solution.py:199
  336.0 217.4 %all-gather.21.cloned.1.call-start = ((), (), s32[]{:S(2)}) async-start(), calls=%async_computation.5 | async-start | bytes 12255232 | tf_op jit(solution)/shard_map/all_gather | solution.py:200
  336.8 314.0 %all-gather.23.cloned.1.call-start = ((), (), s32[]{:S(2)}) async-start(), calls=%async_computation.6 | async-start | bytes 12255232 | tf_op jit(solution)/shard_map/all_gather | solution.py:201
  337.5 357.1 %reduce-scatter.5.cloned.1.call-start = ((), (), s32[]{:S(2)}) async-start(), calls=%async_computation.7 | async-start | bytes 2359296 | tf_op jit(solution)/shard_map/reduce_scatter | solution.py:243
  362.6 288.2 %copy-start.53 = (bf16[384,2048]{1,0:T(8,128)(2,1)S(1)}, bf16[384,2048]{1,0:T(8,128)(2,1)}, u32[]{:S(2)}) copy-start(bf16[384,2048]{1,0:T(8,128)(2,1)} %all-gather.17.cloned.1.call-done) | copy-start | bytes 4718596
  (32 other events, 179.7 us)
Sparse Core Ops, SparseCore 0:
  20.8 44.2 all-gather.28
  67.3 49.2 all-gather.30
  118.8 39.9 all-gather.24
  160.8 49.2 all-gather.26
  290.5 41.7 reduce-scatter.2
  335.4 27.1 all-gather.16
  364.9 93.9 all-gather.18
  461.2 92.2 all-gather.20
  555.6 95.1 all-gather.22
  670.2 24.3 reduce-scatter.4
where the time goes:
time: 712 us; the launch traced here: 704 us
  waiting for transfers between devices  385 us (54%)
  blocking collectives  81.3 us (11%)
  other arithmetic  80.3 us (11%)
  local copies, waits for them, and re-layouts  70.4 us (10%)
  matrix products  70.3 us (10%)
  between operations  14.7 us (2%)
    all_gather x1, waiting for transfers between devices, body(): lax.all_gather(mlp_down, 'sp', axis=1, tiled=True)  97.3 us
    all_gather x1, waiting for transfers between devices, body(): lax.all_gather(mlp_gate, 'sp', axis=0, tiled=True)  96.3 us
    all_gather x1, waiting for transfers between devices, body(): lax.all_gather(mlp_up, 'sp', axis=0, tiled=True)  83.1 us
    all_gather x4, blocking collectives, prefix(): pieces = jax.tree.map(lambda part: lax.all_gather(part, axis), value)  81.3 us
    select_n x60, other arithmetic, hop(): jnp.where(position < mine, new, old)  61.4 us
    reduce_scatter x1, waiting for transfers between devices, body(): lax.psum_scatter(jnp.dot(narrow_out, out_weight[0], preferred_element_typ...  41.9 us
    all_gather x1, waiting for transfers between devices, body(): lax.all_gather(rms_scale(middle, norm_gain), 'tp', axis=0, tiled=True)  24.9 us
    reduce_scatter x1, waiting for transfers between devices, body(): lax.psum_scatter(jnp.dot(hidden, full_down, preferred_element_type=jnp.fl...  24.5 us
  transfers between devices with their start and end apart: 10, of which 7 were waited for; matrix products, arithmetic and copies ran while one was open for 15% of the time, Pallas kernels for 0%

commit v1 on v0

v1 whole, which is shorter than its diff:
```python
import jax
import jax.numpy as jnp
from jax import lax
from jax.sharding import PartitionSpec as P

NORM_EPSILON = 1e-06
ROPE_BASE = 10000.0
BF = jnp.bfloat16
F32 = jnp.float32


def rope_tables(positions, key_size):
    half = key_size // 2
    frequencies = jnp.power(ROPE_BASE, -(jnp.arange(half, dtype=F32) / half))
    angles = positions[:, None] * frequencies[None, :]
    return jnp.cos(angles)[None], jnp.sin(angles)[None]


def rotate(rows, tables):
    cosine, sine = tables
    half = rows.shape[-1] // 2
    a, b = rows[..., :half], rows[..., half:]
    return jnp.concatenate([a * cosine - b * sine, a * sine + b * cosine], -1)


def heads_first(rows, heads):
    return rows.reshape(rows.shape[0], heads, -1).transpose(1, 0, 2)


def local_part(query_rows, key_rows, value_rows, rate_fwd, rate_bwd, positions):
    length = query_rows.shape[0]
    heads = rate_fwd.shape[0]
    key_size = query_rows.shape[1] // heads
    tables = rope_tables(positions, key_size)
    q = rotate(heads_first(query_rows, heads).astype(F32), tables).astype(BF)
    k = (rotate(heads_first(key_rows, heads).astype(F32), tables) * key_size ** (-0.5)).astype(BF)
    v = heads_first(value_rows, heads)
    step = jnp.arange(length, dtype=F32)
    k32 = k.astype(F32)
    k_fwd = (k32 * jnp.exp(rate_fwd[:, None] * (length - 1.0 - step)[None])[..., None]).astype(BF)
    k_bwd = (k32 * jnp.exp(rate_bwd[:, None] * step[None])[..., None]).astype(BF)
    keys = jnp.concatenate([k_fwd, k_bwd], -1)
    state = jnp.einsum("hsk,hsv->hkv", keys, v, preferred_element_type=F32).astype(BF)
    return q, k, v, state


def inside_part(q, k, v, rate_fwd, rate_bwd):
    length = q.shape[1]
    step = jnp.arange(length, dtype=F32)
    offset = (step[:, None] - step[None, :])[None]
    power = jnp.where(offset > 0, rate_fwd[:, None, None], -rate_bwd[:, None, None]) * offset
    weight = jnp.where(offset == 0, 2.0, jnp.exp(power))
    scores = jnp.einsum("htk,hsk->hts", q, k, preferred_element_type=F32)
    return jnp.einsum("hts,hsv->htv", (scores * weight).astype(BF), v, preferred_element_type=F32)


def finish(q, inside, enter, rate_fwd, rate_bwd, gate_rows):
    heads, length, _ = q.shape
    step = jnp.arange(length, dtype=F32)
    q32 = q.astype(F32)
    q_fwd = (q32 * jnp.exp(rate_fwd[:, None] * (step + 1.0)[None])[..., None]).astype(BF)
    q_bwd = (q32 * jnp.exp(rate_bwd[:, None] * (length - step)[None])[..., None]).astype(BF)
    both = jnp.concatenate([q_fwd, q_bwd], -1)
    ret = inside + jnp.einsum("htk,hkv->htv", both, enter, preferred_element_type=F32)
    centred = ret - jnp.mean(ret, -1, keepdims=True)
    variance = jnp.mean(centred * centred, -1, keepdims=True)
    scaled = centred * lax.rsqrt(variance + NORM_EPSILON)
    gated = jax.nn.silu(heads_first(gate_rows, heads).astype(F32)) * scaled
    return gated.astype(BF).transpose(1, 0, 2).reshape(length, -1)


def exchange_states(packed, rates, is_fwd, length):
    count, me = lax.axis_size("sp"), lax.axis_index("sp")
    rows, width = packed.shape
    share = rows // count
    got = lax.all_to_all(packed.reshape(count, share, width), "sp", 0, 0)
    rate = lax.dynamic_slice_in_dim(rates, me * share, share)
    fwd = lax.dynamic_slice_in_dim(is_fwd, me * share, share)
    index = jnp.arange(count, dtype=F32)
    gap = (index[:, None] - index[None, :])[:, :, None]
    gap = jnp.where(fwd[None, None, :] > 0, gap, -gap)
    factor = jnp.where(gap > 0, jnp.exp(rate * length * jnp.maximum(gap - 1.0, 0.0)), 0.0)
    got32 = got.astype(F32)
    entering = jnp.zeros((count, share, width), F32)
    for j in range(count):
        entering += factor[:, j, :, None] * got32[j][None]
    entering = entering.astype(BF)
    return lax.all_to_all(entering, "sp", 0, 0).reshape(rows, width)


def shift_tp(array, by):
    count = lax.axis_size("tp")
    return lax.ppermute(array, "tp", [((i + by) % count, i) for i in range(count)])


def from_all(array):
    return [array] + [shift_tp(array, by) for by in range(1, lax.axis_size("tp"))]


def in_order(pieces):
    count, me = len(pieces), lax.axis_index("tp")
    ordered = []
    for place in range(count):
        piece = pieces[0]
        for ahead in range(1, count):
            piece = jnp.where((me + ahead) % count == place, pieces[ahead], piece)
        ordered.append(piece)
    return jnp.concatenate(ordered, 0)


def body(
    stream,
    query_narrow,
    key_narrow,
    query_wide,
    key_wide,
    values,
    out_gate,
    out_weight,
    norm_gain,
    mlp_gate,
    mlp_up,
    mlp_down,
    log_decay,
):
    tp = lax.axis_index("tp")
    full_gate = lax.all_gather(mlp_gate, "sp", axis=0, tiled=True)
    full_up = lax.all_gather(mlp_up, "sp", axis=0, tiled=True)
    full_down = lax.all_gather(mlp_down, "sp", axis=1, tiled=True)
    weights = from_all(out_weight.reshape(-1, out_weight.shape[-1]))
    stream_rows = in_order(from_all(stream))

    length = query_narrow.shape[0]
    positions = (lax.axis_index("sp") * length + jnp.arange(length, dtype=jnp.int32)).astype(F32)
    queries, keys = (query_narrow, query_wide), (key_narrow, key_wide)
    parts, states, rates, is_fwd = [], [], [], []
    for g in range(2):
        fwd, bwd = log_decay[0, g], log_decay[1, g]
        q, k, v, state = local_part(queries[g], keys[g], values[:, g], fwd, bwd, positions)
        parts.append((q, k, v, fwd, bwd))
        states.append(state)
        heads, key_size = q.shape[0], q.shape[2]
        rates.append(jnp.repeat(jnp.stack([fwd, bwd], 1).reshape(-1), key_size))
        is_fwd.append(jnp.tile(jnp.repeat(jnp.array([1.0, 0.0], F32), key_size), heads))
    width = states[0].shape[-1]
    packed = jnp.concatenate([s.reshape(-1, width) for s in states], 0)
    entering = exchange_states(packed, jnp.concatenate(rates), jnp.concatenate(is_fwd), float(length))
    outs, at = [], 0
    for g in range(2):
        q, k, v, fwd, bwd = parts[g]
        size = states[g].shape[0] * states[g].shape[1]
        enter = entering[at : at + size].reshape(states[g].shape)
        at += size
        inside = inside_part(q, k, v, fwd, bwd)
        outs.append(finish(q, inside, enter, fwd, bwd, out_gate[:, g]))
    ys = from_all(jnp.concatenate(outs, 1))
    proj = jnp.dot(ys[0], weights[0], preferred_element_type=F32)
    for y, weight in zip(ys[1:], weights[1:]):
        proj += jnp.dot(y, weight, preferred_element_type=F32)
    middle = (stream_rows.astype(F32) + proj).astype(BF)
    wide = middle.astype(F32)
    normed = (
        wide * lax.rsqrt(jnp.mean(wide * wide, -1, keepdims=True) + NORM_EPSILON) * norm_gain
    ).astype(BF)
    gate_act = jnp.dot(normed, full_gate, preferred_element_type=F32)
    up_act = jnp.dot(normed, full_up, preferred_element_type=F32)
    hidden = (jax.nn.silu(gate_act) * up_act).astype(BF)
    rows, count = stream.shape[0], lax.axis_size("tp")
    down = 0.0
    for by in list(range(1, count)) + [0]:
        start = ((tp + by) % count) * rows
        part = jnp.dot(
            lax.dynamic_slice_in_dim(hidden, start, rows), full_down, preferred_element_type=F32
        )
        down += shift_tp(part.astype(BF), count - by).astype(F32) if by else part
    middle_mine = lax.dynamic_slice_in_dim(middle, tp * rows, rows)
    return (middle_mine.astype(F32) + 0.5 * down).astype(BF)


def solution(mesh):
    return jax.shard_map(
        body,
        mesh=mesh,
        in_specs=(
            P(("sp", "tp"), None),
            P("sp", "tp"),
            P("sp", "tp"),
            P("sp", "tp"),
            P("sp", "tp"),
            P("sp", None, "tp"),
            P("sp", None, "tp"),
            P(None, "tp", None),
            P(),
            P("sp", "tp"),
            P("sp", "tp"),
            P("tp", "sp"),
            P(None, None, "tp"),
        ),
        out_specs=P(("sp", "tp"), None),
        check_vma=False,
    )
```

time: 712 us -> 356 us (0.50)
  waiting for transfers between devices: 385 us -> 238 us
  blocking collectives: 81.3 us -> 0 us
  other arithmetic: 80.3 us -> 18.4 us
  local copies, waits for them, and re-layouts: 70.4 us -> 10.9 us
  starting transfers between devices: 0.76 us -> 20.6 us
  matrix products: 70.3 us -> 53.3 us
    all_gather x8 -> x3, waiting for transfers between devices: 316 us -> 132 us  [the longest x1 86.3 us: body(): full_down = lax.all_gather(mlp_down, 'sp', axis=1, tiled=True)]
    ppermute x0 -> x4, waiting for transfers between devices: none -> 87.1 us  [shift_tp(): lax.ppermute(array, 'tp', [((i + by) % count, i) for i in range(count)])]
    all_gather x4 -> x0, blocking collectives: 81.3 us -> none  [prefix(): pieces = jax.tree.map(lambda part: lax.all_gather(part, axis), value)]
    reduce_scatter x2 -> x0, waiting for transfers between devices: 66.4 us -> none  [the longest x1 41.9 us: body(): lax.psum_scatter(jnp.dot(narrow_out, out_weight[0], preferred_element_typ...]
    select_n x61 -> x2, other arithmetic: 62.5 us -> 2.3 us  [the longest x1 1.51 us: in_order(): piece = jnp.where((me + ahead) % count == place, pieces[ahead], piece)]
    mul x34 -> x2, local copies, waits for them, and re-layouts: 23.3 us -> 0.94 us  [exchange_states(): entering += factor[:, j, :, None] * got32[j][None]]
    dot_general x22 -> x12, matrix products: 70.3 us -> 53.3 us  [the longest x2 15.1 us: body(): jnp.dot(lax.dynamic_slice_in_dim(hidden, start, rows), full_down, preferr...]
    all_to_all x0 -> x2, waiting for transfers between devices: none -> 16.7 us  [the longest x1 9.73 us: exchange_states(): return lax.all_to_all(entering, 'sp', 0, 0).reshape(rows, width)]
  transfers between devices with their start and end apart: 10 -> 9, of which waited for: 7 -> 6; matrix products, arithmetic and copies ran while one was open for 15% -> 19% of each run, Pallas kernels for 0% -> 0%
where the time goes in v1:
time: 356 us; the launch traced here: 355 us
  waiting for transfers between devices  238 us (67%)
  matrix products  53.3 us (15%)
  starting transfers between devices  20.6 us (6%)
  other arithmetic  18.4 us (5%)
  between operations  13.6 us (4%)
  local copies, waits for them, and re-layouts  10.9 us (3%)
    ppermute x4, waiting for transfers between devices, shift_tp(): lax.ppermute(array, 'tp', [((i + by) % count, i) for i in range(count)])  87.1 us
    all_gather x1, waiting for transfers between devices, body(): full_down = lax.all_gather(mlp_down, 'sp', axis=1, tiled=True)  86.3 us
    all_gather x1, waiting for transfers between devices, body(): full_up = lax.all_gather(mlp_up, 'sp', axis=0, tiled=True)  46.1 us
    dot_general x2, matrix products, body(): jnp.dot(lax.dynamic_slice_in_dim(hidden, start, rows), full_down, preferr...  15.1 us
    dot_general x1, matrix products, body(): up_act = jnp.dot(normed, full_up, preferred_element_type=F32)  11.1 us
    dot_general x1, matrix products, body(): gate_act = jnp.dot(normed, full_gate, preferred_element_type=F32)  10.2 us
    all_to_all x1, waiting for transfers between devices, exchange_states(): return lax.all_to_all(entering, 'sp', 0, 0).reshape(rows, width)  9.73 us
    all_to_all x1, starting transfers between devices, exchange_states(): return lax.all_to_all(entering, 'sp', 0, 0).reshape(rows, width)  7.86 us
  transfers between devices with their start and end apart: 9, of which 6 were waited for; matrix products, arithmetic and copies ran while one was open for 19% of the time, Pallas kernels for 0%

profile of v1, /device:TPU:0, one launch (start us, length us, event | category | flops | bytes accessed | tf_op | source)
XLA Modules:
  0.0 355.0 jit_solution(10380373230757094244)
XLA Ops:
  8.8 1.1 copy.49
  10.0 1.1 fusion.88
  11.1 1.7 copy.51
  12.9 1.2 copy.63
  14.7 0.9 copy.57
  18.9 1.0 multiply_subtract_fusion
  21.2 7.4 %all-to-all-start = ((bf16[16,96,128]{2,1,0:T(8,128)(2,1)}), bf16[16,96,128]{2,1,0:T(8,128)(2,1)S(1)}, u32[]{:S(2)}, u32[]{:S(2)}) async-start(bf16[16,96,128]{2,1,0:T(8,128)(2,1)} %bitcast.28), calls=%async_computation | async-start | bytes 786432 | tf_op jit(solution)/shard_map/all_to_all | solution.py:76
  28.6 1.6 collective-permute-start
  33.1 1.1 fusion.87
  36.7 1.8 fusion.43
  38.5 2.0 fusion.23
  40.5 6.9 %all-to-all-done = bf16[16,96,128]{2,1,0:T(8,128)(2,1)S(1)} async-done(((bf16[16,96,128]{2,1,0:T(8,128)(2,1)}), bf16[16,96,128]{2,1,0:T(8,128)(2,1)S(1)}, u32[]{:S(2)}, u32[]{:S(2)}) %all-to-all-start) | async-done | bytes 393248 | tf_op jit(solution)/shard_map/all_to_all | solution.py:76
  47.6 4.5 %add_convert_fusion.2 = bf16[16,96,128]{2,1,0:T(8,128)(2,1)} fusion(f32[96,128]{1,0:T(8,128)S(1)} %get-tuple-element.14, f32[16,96]{1,0:T(8,128)S(1)} %get-tuple-element.46, f32[96,128]{1,0:T(8,128)S(1)} %get-tuple-element.15, f32[16,96]{1,0:T(8,128)S(1)} %get-tuple-element.47, f32[96,128]{1,0:T(8,128)S(1)} %get-tuple-element.16, ...), kind=kLoop, calls=%fused_computation.60 | loop fusion | flops 6291456 | bytes 1277952 | tf_op jit(solution)/shard_map/convert_element_type | solution.py:87
  52.1 7.9 %all-to-all-start.1 = ((bf16[16,96,128]{2,1,0:T(8,128)(2,1)}), bf16[16,96,128]{2,1,0:T(8,128)(2,1)S(1)}, u32[]{:S(2)}, u32[]{:S(2)}) async-start(bf16[16,96,128]{2,1,0:T(8,128)(2,1)} %add_convert_fusion.2), calls=%async_computation.1 | async-start | bytes 786432 | tf_op jit(solution)/shard_map/all_to_all | solution.py:88
  59.9 0.9 fusion.38
  60.9 4.4 %fusion.4 = f32[4,384,128]{1,2,0:T(8,128)} fusion(bf16[4,384,128]{1,2,0:T(8,128)(2,1)} %bitcast.179, f32[384,384]{1,0:T(8,128)} %iota_subtract_fusion, f32[4]{0:T(128)S(1)} %copy-done.27, f32[4]{0:T(128)S(1)} %copy-done.21, pred[384,384]{1,0:T(8,128)(4,1)} %get-tuple-element.103, pred[384,384]{1,0:T(8,128)(4,1)} %get-tuple-element.104, ...), kind=kOutput, calls=%fused_computation.12 | convolution fusion | flops 230129664 | bytes 2654240 | tf_op jit(solution)/shard_map/hts,hsv->htv/dot_general | solution.py:54
  65.4 3.4 fusion.5
  68.8 9.7 %all-to-all-done.1 = bf16[16,96,128]{2,1,0:T(8,128)(2,1)S(1)} async-done(((bf16[16,96,128]{2,1,0:T(8,128)(2,1)}), bf16[16,96,128]{2,1,0:T(8,128)(2,1)S(1)}, u32[]{:S(2)}, u32[]{:S(2)}) %all-to-all-start.1) | async-done | bytes 393248 | tf_op jit(solution)/shard_map/all_to_all | solution.py:88
  78.6 1.7 fusion.90
  81.5 1.6 collective-permute-start.1
  83.2 1.5 broadcast_select_fusion.1
  84.7 1.9 fusion.84
  86.6 68.9 %collective-permute-done.1 = bf16[384,1024]{0,1:T(8,128)(2,1)S(1)} collective-permute-done((bf16[384,1024]{0,1:T(8,128)(2,1)S(1)}, bf16[384,1024]{0,1:T(8,128)(2,1)S(1)}, u32[]{:S(2)}, u32[]{:S(2)}) %collective-permute-start.1) | collective-permute-done | bytes 786464 | tf_op jit(solution)/shard_map/ppermute | solution.py:93
  155.4 4.5 %fusion.1 = (f32[384]{0:T(512)S(1)}, bf16[384,2048]{1,0:T(8,128)(2,1)S(1)}) fusion(f32[384,2048]{1,0:T(8,128)S(1)} %fusion.84, bf16[384,1024]{0,1:T(8,128)(2,1)S(1)} %collective-permute-done.1, bf16[1024,2048]{1,0:T(8,128)(2,1)} %collective-permute-done.2, bf16[192,2048]{1,0:T(8,128)(2,1)S(1)} %get-tuple-element.6, bf16[192,2048]{1,0:T(8,128)(2,1)S(1)} %get-tuple-element.5), kind=kOutput, calls=%fused_computation.4 | convolution fusion | flops 1618476672 | bytes 11273728 | tf_op jit(solution)/shard_map/dot_general | solution.py:159
  159.9 10.2 %fusion.41 = f32[384,2816]{1,0:T(8,128)} fusion(bf16[2048,2816]{1,0:T(8,128)(2,1)} %all-gather.4.cloned.1.call-done, bf16[384,2048]{1,0:T(8,128)(2,1)S(1)} %get-tuple-element.96, f32[2048]{0:T(1024)S(1)} %copy-done.28, f32[384]{0:T(512)S(1)} %add_rsqrt_fusion), kind=kOutput, calls=%fused_computation.70 | convolution fusion | flops 4432330752 | bytes 17442304 | tf_op jit(solution)/shard_map/dot_general | solution.py:165
  170.2 46.1 %all-gather.6.cloned.1.call-done = bf16[2048,2816]{1,0:T(8,128)(2,1)} async-done(((bf16[128,2816]{1,0:T(8,128)(2,1)}), bf16[2048,2816]{1,0:T(8,128)(2,1)}) %all-gather.6.cloned.1.call-update) | async-done | bytes 11534352 | tf_op jit(solution)/shard_map/all_gather | solution.py:128
  216.2 11.1 %fusion = bf16[384,2816]{1,0:T(8,128)(2,1)} fusion(bf16[2048,2816]{1,0:T(8,128)(2,1)} %all-gather.6.cloned.1.call-done, f32[384,2816]{1,0:T(8,128)} %fusion.41, bf16[384,2048]{1,0:T(8,128)(2,1)S(1)} %get-tuple-element.96, f32[2048]{0:T(1024)S(1)} %copy-done.28, f32[384]{0:T(512)S(1)} %add_rsqrt_fusion), kind=kOutput, calls=%fused_computation.1 | convolution fusion | flops 4438818816 | bytes 19604992 | tf_op jit(solution)/shard_map/dot_general | solution.py:166
  227.3 86.3 %all-gather.8.cloned.1.call-done = bf16[2816,2048]{1,0:T(8,128)(2,1)} async-done(((bf16[2816,128]{1,0:T(8,128)(2,1)}), bf16[2816,2048]{1,0:T(8,128)(2,1)}) %all-gather.8.cloned.1.call-update) | async-done | bytes 11534352 | tf_op jit(solution)/shard_map/all_gather | solution.py:129
  313.6 7.1 %convolution_convert_fusion = bf16[192,2048]{1,0:T(8,128)(2,1)S(1)} fusion(bf16[2816,2048]{1,0:T(8,128)(2,1)} %all-gather.8.cloned.1.call-done, bf16[384,2816]{1,0:T(8,128)(2,1)} %fusion, s32[]{:T(128)S(6)} %select_n.77), kind=kOutput, calls=%fused_computation.8 | convolution fusion | flops 2214985728 | bytes 13402116 | tf_op jit(solution)/shard_map/dot_general | solution.py:172
  320.6 1.5 collective-permute-start.3
  322.2 18.2 %collective-permute-done.3 = bf16[192,2048]{1,0:T(8,128)(2,1)S(1)} collective-permute-done((bf16[192,2048]{1,0:T(8,128)(2,1)S(1)}, bf16[192,2048]{1,0:T(8,128)(2,1)S(1)}, u32[]{:S(2)}, u32[]{:S(2)}) %collective-permute-start.3) | collective-permute-done | bytes 786464 | tf_op jit(solution)/shard_map/ppermute | solution.py:93
  340.4 8.1 %add_convert_fusion.1 = bf16[192,2048]{1,0:T(8,128)(2,1)} fusion(bf16[192,2048]{1,0:T(8,128)(2,1)S(1)} %collective-permute-done.3, bf16[384,2048]{1,0:T(8,128)(2,1)S(1)} %get-tuple-element.96, s32[]{:T(128)S(6)} %select_n.76, bf16[2816,2048]{1,0:T(8,128)(2,1)} %all-gather.8.cloned.1.call-done, bf16[384,2816]{1,0:T(8,128)(2,1)} %fusion, s32[]{:T(128)S(6)} %select_n.79), kind=kOutput, calls=%fused_computation.11 | convolution fusion | flops 2216951808 | bytes 14974984 | tf_op jit(solution)/shard_map/dot_general | solution.py:172
  (128 shorter events, 14.4 us)
Async XLA Ops:
  6.5 3.3 copy-start.15
  6.5 3.4 copy-start.1
  6.5 153.4 %all-gather.4.cloned.1.call-start = ((), (), s32[]{:S(2)}) async-start(), calls=%async_computation.2 | async-start | bytes 12255232 | tf_op jit(solution)/shard_map/all_gather | solution.py:127
  7.3 209.0 %all-gather.6.cloned.1.call-start = ((), (), s32[]{:S(2)}) async-start(), calls=%async_computation.3 | async-start | bytes 12255232 | tf_op jit(solution)/shard_map/all_gather | solution.py:128
  8.0 305.6 %all-gather.8.cloned.1.call-start = ((), (), s32[]{:S(2)}) async-start(), calls=%async_computation.4 | async-start | bytes 12255232 | tf_op jit(solution)/shard_map/all_gather | solution.py:129
  12.7 2.9 copy-start.16
  15.6 2.9 copy-start.14
  19.8 10.9 %copy-start.22 = (f32[4,1]{0,1:T(1,128)S(1)}, f32[4,1]{0,1:T(1,128)}, u32[]{:S(2)}) copy-start(f32[4,1]{0,1:T(1,128)} %get-tuple-element.77) | copy-start | bytes 52
  19.8 10.9 %copy-start.23 = (f32[4,1]{0,1:T(1,128)S(1)}, f32[4,1]{0,1:T(1,128)}, u32[]{:S(2)}) copy-start(f32[4,1]{0,1:T(1,128)} %get-tuple-element.78) | copy-start | bytes 52
  19.9 10.8 %copy-start.24 = (f32[4,1]{0,1:T(1,128)S(1)}, f32[4,1]{0,1:T(1,128)}, u32[]{:S(2)}) copy-start(f32[4,1]{0,1:T(1,128)} %get-tuple-element.83) | copy-start | bytes 52
  19.9 10.8 %copy-start.25 = (f32[4,1]{0,1:T(1,128)S(1)}, f32[4,1]{0,1:T(1,128)}, u32[]{:S(2)}) copy-start(f32[4,1]{0,1:T(1,128)} %get-tuple-element.84) | copy-start | bytes 52
  19.9 11.4 %copy-start.29 = (f32[2]{0:T(128)S(1)}, f32[2]{0:T(128)}, u32[]{:S(2)}) copy-start(f32[2]{0:T(128)} %constant.90.clone) | copy-start | bytes 28
  19.9 11.8 %copy-start.17 = (f32[2,2,4]{2,1,0:T(2,128)S(1)}, f32[2,2,4]{2,1,0:T(2,128)}, u32[]{:S(2)}) copy-start(f32[2,2,4]{2,1,0:T(2,128)} %param.27) | copy-start | bytes 196
  19.9 13.2 %copy-start.2 = (bf16[384,2,512]{2,1,0:T(2,128)(2,1)S(1)}, bf16[384,2,512]{2,1,0:T(2,128)(2,1)}, u32[]{:S(2)}) copy-start(bf16[384,2,512]{2,1,0:T(2,128)(2,1)} %param.21) | copy-start | bytes 2359300
  21.2 26.3 %all-to-all-start = ((bf16[16,96,128]{2,1,0:T(8,128)(2,1)}), bf16[16,96,128]{2,1,0:T(8,128)(2,1)S(1)}, u32[]{:S(2)}, u32[]{:S(2)}) async-start(bf16[16,96,128]{2,1,0:T(8,128)(2,1)} %bitcast.28), calls=%async_computation | async-start | bytes 786432 | tf_op jit(solution)/shard_map/all_to_all | solution.py:76
  28.6 54.6 %collective-permute-start = (bf16[192,2048]{1,0:T(8,128)(2,1)}, bf16[192,2048]{1,0:T(8,128)(2,1)}, u32[]{:S(2)}, u32[]{:S(2)}) collective-permute-start(bf16[192,2048]{1,0:T(8,128)(2,1)} %param.15), channel_id=1, source_target_pairs={{1,0},{0,1},{3,2},{2,3},{5,4},{4,5},{7,6},{6,7},{9,8},{8,9},{11,10... | collective-permute-start | bytes 2359304 | tf_op jit(solution)/shard_map/ppermute | solution.py:93
  30.2 125.2 %collective-permute-start.2 = (bf16[1024,2048]{1,0:T(8,128)(2,1)}, bf16[1024,2048]{1,0:T(8,128)(2,1)}, u32[]{:S(2)}, u32[]{:S(2)}) collective-permute-start(bf16[1024,2048]{1,0:T(8,128)(2,1)} %bitcast.161), channel_id=1, source_target_pairs={{1,0},{0,1},{3,2},{2,3},{5,4},{4,5},{7,6},{6,7},{9,8},{8,9},{11,10... | collective-permute-start | bytes 12582920 | tf_op jit(solution)/shard_map/ppermute | solution.py:93
  40.5 20.4 %copy-start.21 = (f32[4]{0:T(128)S(1)}, f32[4]{0:T(128)}, u32[]{:S(2)}) copy-start(f32[4]{0:T(128)} %copy-done.20) | copy-start | bytes 52
  40.5 20.4 %copy-start.27 = (f32[4]{0:T(128)S(1)}, f32[4]{0:T(128)}, u32[]{:S(2)}) copy-start(f32[4]{0:T(128)} %get-tuple-element.75) | copy-start | bytes 52
  52.1 26.4 %all-to-all-start.1 = ((bf16[16,96,128]{2,1,0:T(8,128)(2,1)}), bf16[16,96,128]{2,1,0:T(8,128)(2,1)S(1)}, u32[]{:S(2)}, u32[]{:S(2)}) async-start(bf16[16,96,128]{2,1,0:T(8,128)(2,1)} %add_convert_fusion.2), calls=%async_computation.1 | async-start | bytes 786432 | tf_op jit(solution)/shard_map/all_to_all | solution.py:88
  60.9 4.5 %copy-start.4 = (f32[4,384,64]{1,2,0:T(8,128)S(1)}, f32[4,384,64]{1,2,0:T(8,128)}, u32[]{:S(2)}) copy-start(f32[4,384,64]{1,2,0:T(8,128)} %copy-done.3) | copy-start | bytes 1179652
  60.9 4.5 %copy-start.7 = (bf16[4,384,64]{1,2,0:T(8,128)(2,1)S(1)}, bf16[4,384,64]{1,2,0:T(8,128)(2,1)}, u32[]{:S(2)}) copy-start(bf16[4,384,64]{1,2,0:T(8,128)(2,1)} %get-tuple-element.43) | copy-start | bytes 589828
  60.9 4.5 %copy-start.8 = (bf16[4,384,64]{1,2,0:T(8,128)(2,1)S(1)}, bf16[4,384,64]{1,2,0:T(8,128)(2,1)}, u32[]{:S(2)}) copy-start(bf16[4,384,64]{1,2,0:T(8,128)(2,1)} %get-tuple-element.44) | copy-start | bytes 589828
  60.9 4.5 %copy-start.19 = (f32[4]{0:T(128)S(1)}, f32[4]{0:T(128)}, u32[]{:S(2)}) copy-start(f32[4]{0:T(128)} %copy-done.18) | copy-start | bytes 52
  60.9 4.5 %copy-start.26 = (f32[4]{0:T(128)S(1)}, f32[4]{0:T(128)}, u32[]{:S(2)}) copy-start(f32[4]{0:T(128)} %get-tuple-element.76) | copy-start | bytes 52
  68.8 11.6 %copy-start.5 = (bf16[4,384,128]{1,2,0:T(8,128)(2,1)S(1)}, bf16[4,384,128]{1,2,0:T(8,128)(2,1)}, u32[]{:S(2)}) copy-start(bf16[4,384,128]{1,2,0:T(8,128)(2,1)} %get-tuple-element.37) | copy-start | bytes 1179652
  68.8 11.6 %copy-start.6 = (bf16[4,384,128]{1,2,0:T(8,128)(2,1)S(1)}, bf16[4,384,128]{1,2,0:T(8,128)(2,1)}, u32[]{:S(2)}) copy-start(bf16[4,384,128]{1,2,0:T(8,128)(2,1)} %get-tuple-element.38) | copy-start | bytes 1179652
  68.8 11.6 %copy-start.9 = (f32[4,384,128]{1,2,0:T(8,128)S(1)}, f32[4,384,128]{1,2,0:T(8,128)}, u32[]{:S(2)}) copy-start(f32[4,384,128]{1,2,0:T(8,128)} %fusion.5) | copy-start | bytes 2359300
  81.4 3.3 copy-start
  81.5 73.9 %collective-permute-start.1 = (bf16[384,1024]{0,1:T(8,128)(2,1)S(1)}, bf16[384,1024]{0,1:T(8,128)(2,1)S(1)}, u32[]{:S(2)}, u32[]{:S(2)}) collective-permute-start(bf16[384,1024]{0,1:T(8,128)(2,1)S(1)} %pad_maximum_fusion), channel_id=1, source_target_pairs={{1,0},{0,1},{3,2},{2,3},{5,4},{4,5},{7,6},{6,7},{9,8},{8,9},{11,10... | collective-permute-start | bytes 2359304 | tf_op jit(solution)/shard_map/ppermute | solution.py:93
  155.4 4.5 %copy-start.28 = (f32[2048]{0:T(1024)S(1)}, f32[2048]{0:T(1024)}, u32[]{:S(2)}) copy-start(f32[2048]{0:T(1024)} %param.23) | copy-start | bytes 24580
  320.6 19.8 %collective-permute-start.3 = (bf16[192,2048]{1,0:T(8,128)(2,1)S(1)}, bf16[192,2048]{1,0:T(8,128)(2,1)S(1)}, u32[]{:S(2)}, u32[]{:S(2)}) collective-permute-start(bf16[192,2048]{1,0:T(8,128)(2,1)S(1)} %convolution_convert_fusion), channel_id=1, source_target_pairs={{1,0},{0,1},{3,2},{2,3},{5,4},{4,5},{7,6},{6,7},{9,8},{8,9},{11,10... | collective-permute-start | bytes 2359304 | tf_op jit(solution)/shard_map/ppermute | solution.py:93
  (7 other events, 12.6 us)
Sparse Core Ops, SparseCore 0:
  9.6 111.1 all-gather.3
  123.1 93.0 all-gather.5
  218.4 95.1 all-gather.7
